TPU v7x, 32 devices: a whole 2x2x4 slice. The times are simulated.
32 devices in a mesh: kv: 8 (over z, y), tp: 4 (over x, core).
Axes of the slice: x: 2, y: 2, z: 4, core: 2. Of those that a mesh axis runs over, the one named last changes fastest.
Arguments:
- tokens: bfloat16 [256, 4, 2048], P(None, None, ('kv', 'tp')), may hold values from -520 to 520
- input_norm_gain: bfloat16 [2048], replicated, may hold values from 0.099609375 to 1.8984375
- query_weight: bfloat16 [2048, 2048], P(None, 'kv'), may hold values from -0.125 to 0.125
- key_weight: bfloat16 [2048, 2048], P(None, 'kv'), may hold values from -0.125 to 0.125
- value_weight: bfloat16 [2048, 16, 128], P(None, 'kv', 'tp'), may hold values from -1.14904852 to 1.14904852
- output_gate_weight: bfloat16 [2048, 16, 128], P(None, 'kv', 'tp'), may hold values from -0.125 to 0.125
- strength_weight: bfloat16 [2048, 16], P(None, 'kv'), may hold values from -0.125 to 0.125
- decay_weight: bfloat16 [2048, 16], P(None, 'kv'), may hold values from -0.125 to 0.125
- head_decay_rate: float32 [16], P('kv'), may hold values from 0.005 to 1.5
- proposal_log_decay: float32 [256, 4, 16], P(None, None, 'kv'), may hold values from -0.69 to 0
- head_norm_gain: bfloat16 [128], P('tp'), may hold values from 0.099609375 to 1.8984375
- output_weight: bfloat16 [16, 128, 2048], P('kv', 'tp'), may hold values from -1.14904852 to 1.14904852
- output_norm_gain: bfloat16 [2048], P(('kv', 'tp')), may hold values from 0.099609375 to 1.8984375
- state: float32 [256, 16, 128, 128], P(None, 'kv', 'tp'), may hold values from -4.5961941 to 4.5961941
- previous_keys: bfloat16 [256, 4, 2048], P(None, None, 'kv'), may hold values from -6 to 6
- previous_values: bfloat16 [256, 4, 16, 128], P(None, None, 'kv', 'tp'), may hold values from -52 to 52
- previous_log_decay: float32 [256, 4, 16], P(None, None, 'kv'), may hold values from -0.7 to -0.02
- previous_strengths: float32 [256, 4, 16], P(None, None, 'kv'), may hold values from 0.1 to 0.9
- accepted: int32 [256], replicated, may hold values from 0 to 4
- parent: int32 [256, 4], replicated, may hold values from -1 to 2, as said below
Outputs:
- layer_out: bfloat16 [256, 4, 2048], P(None, None, ('kv', 'tp'))
- accepted_state: float32 [256, 16, 128, 128], P(None, 'kv', 'tp')
Inputs may be any that keep to these rules, and one draw needn't show every extreme that they name: parent[b, i] is -1 or a proposal index below i; -1 means that proposal i follows the accepted old proposals directly.
All inputs are finite; a program needn't handle non-finite values.
Results may differ from a plain program's by a relative error of at most 0.019.
Values may be sent and summed in bfloat16 or wider, within the bound.
A program may use at most 128 MiB of HBM per device.

v0:
```python
import jax
import jax.numpy as jnp
from jax import lax
from jax.sharding import PartitionSpec as P

epsilon = 1e-06


def unit_rows(matrix):
    return matrix * lax.rsqrt(jnp.sum(matrix * matrix, axis=-1, keepdims=True) + epsilon)


def exact_product(form, left, right):
    return jnp.einsum(form, left, right, precision=lax.Precision.HIGHEST)


def visibility(parent):
    sequence_count, proposal_count = parent.shape
    position = jnp.arange(proposal_count, dtype=jnp.int32)
    parent_hot = (parent[:, :, None] == position[None, None, :]).astype(jnp.float32)
    ancestry = []
    for row_index in range(proposal_count):
        ancestor_row = parent_hot[:, row_index, :]
        if row_index > 0:
            earlier = jnp.stack(ancestry, axis=1)
            ancestor_row = ancestor_row + exact_product(
                "bj,bjk->bk", parent_hot[:, row_index, :row_index], earlier
            )
        ancestry.append(ancestor_row)
    ancestor = jnp.stack(ancestry, axis=1)
    chain = (position[:, None] > position[None, :]).astype(jnp.float32)
    upper = jnp.concatenate(
        [
            jnp.broadcast_to(chain, (sequence_count, proposal_count, proposal_count)),
            jnp.zeros((sequence_count, proposal_count, proposal_count), jnp.float32),
        ],
        axis=2,
    )
    lower = jnp.concatenate(
        [jnp.ones((sequence_count, proposal_count, proposal_count), jnp.float32), ancestor], axis=2
    )
    return jnp.concatenate([upper, lower], axis=1)


def split_heads(matrix, sequence_count, proposal_count, number_of_heads):
    return (
        matrix.astype(jnp.float32)
        .reshape(sequence_count, proposal_count, number_of_heads, -1)
        .transpose(0, 2, 1, 3)
    )


def delta_recursion(
    query_projected,
    key_projected,
    value_projected,
    output_gate_logits,
    write_strength_logits,
    decay_logits,
    decay_speed,
    proposal_group,
    head_norm_gain,
    state,
    previous_keys,
    previous_values,
    previous_log_decay,
    previous_strengths,
    accepted,
    parent,
    channel_count_total,
):
    sequence_count, number_of_heads, value_dim, head_dim = state.shape
    proposal_count = parent.shape[1]
    queries = unit_rows(
        split_heads(query_projected, sequence_count, proposal_count, number_of_heads)
    ) * head_dim ** (-0.5)
    new_keys = unit_rows(
        split_heads(key_projected, sequence_count, proposal_count, number_of_heads)
    )
    old_keys = unit_rows(
        split_heads(previous_keys, sequence_count, proposal_count, number_of_heads)
    )
    new_values = split_heads(value_projected, sequence_count, proposal_count, number_of_heads)
    old_values = split_heads(previous_values, sequence_count, proposal_count, number_of_heads)
    zgate = split_heads(output_gate_logits, sequence_count, proposal_count, number_of_heads)
    beta_new = jax.nn.sigmoid(
        write_strength_logits.reshape(sequence_count, proposal_count, number_of_heads)
    ).transpose(0, 2, 1)
    fresh_decay = (
        -decay_speed[None, None, :]
        * jax.nn.softplus(decay_logits.reshape(sequence_count, proposal_count, number_of_heads))
        + proposal_group
    ).transpose(0, 2, 1)
    position = jnp.arange(proposal_count, dtype=jnp.int32)
    live = (position[None, :] < accepted[:, None]).astype(jnp.float32)[:, None, :]
    beta_old = previous_strengths.transpose(0, 2, 1) * live
    decay_old = previous_log_decay.transpose(0, 2, 1) * live
    keys_all = jnp.concatenate([old_keys, new_keys], axis=2)
    values_all = jnp.concatenate([old_values, new_values], axis=2)
    beta_all = jnp.concatenate([beta_old, beta_new], axis=2)
    decay_all = jnp.concatenate([decay_old, fresh_decay], axis=2)
    visible = visibility(parent)
    gamma_sum = decay_all + exact_product("bij,bhj->bhi", visible, decay_all)
    gamma_diff = gamma_sum[:, :, :, None] - gamma_sum[:, :, None, :]
    decay_pair = jnp.exp(jnp.minimum(gamma_diff, 0.0)) * visible[:, None]
    coupling = (
        beta_all[..., None] * exact_product("bhid,bhjd->bhij", keys_all, keys_all) * decay_pair
    )
    right_side = jnp.concatenate(
        [beta_all[..., None] * values_all, (beta_all * jnp.exp(gamma_sum))[..., None] * keys_all],
        axis=-1,
    )
    solved = []
    for row_index in range(2 * proposal_count):
        current = right_side[:, :, row_index]
        if row_index > 0:
            current = current - exact_product(
                "bhj,bhjd->bhd", coupling[:, :, row_index, :row_index], jnp.stack(solved, axis=2)
            )
        solved.append(current)
    solution = jnp.stack(solved, axis=2)
    update = solution[..., :value_dim] - exact_product(
        "bhcd,bhed->bhce", solution[..., value_dim:], state
    )
    identity = jnp.eye(2 * proposal_count, dtype=jnp.float32)
    seen = visible[:, proposal_count:] + identity[proposal_count:][None]
    reach = jnp.exp(jnp.minimum(gamma_diff[:, :, proposal_count:], 0.0)) * seen[:, None]
    query_key = exact_product("bhid,bhjd->bhij", queries, keys_all) * reach
    readout = exact_product(
        "bhid,bhed->bhie", queries * jnp.exp(gamma_sum[:, :, proposal_count:])[..., None], state
    )
    readout = readout + exact_product("bhij,bhje->bhie", query_key, update)
    squares = channel_count_total(jnp.sum(readout * readout, axis=-1))
    readout = readout * lax.rsqrt(squares / head_dim + epsilon)[..., None]
    readout = readout * head_norm_gain.astype(jnp.float32) * jax.nn.silu(zgate)
    blended_rows = readout.transpose(0, 2, 1, 3).reshape(
        sequence_count * proposal_count, number_of_heads * value_dim
    )
    blended_rows = blended_rows.astype(jnp.bfloat16)
    last_gamma = gamma_sum[:, :, proposal_count - 1 : proposal_count]
    key_weighted = old_keys * jnp.exp(last_gamma - gamma_sum[:, :, :proposal_count])[..., None]
    accepted_state = jnp.exp(last_gamma)[..., None] * state + exact_product(
        "bhcd,bhce->bhed", key_weighted, update[:, :, :proposal_count]
    )
    return (blended_rows, accepted_state)


def channel_sum(squares):
    return lax.psum(squares, "tp")


def on_device(
    tokens,
    input_norm_gain,
    query_weight,
    key_weight,
    value_weight,
    output_gate_weight,
    strength_weight,
    decay_weight,
    head_decay_rate,
    proposal_log_decay,
    head_norm_gain,
    output_weight,
    output_norm_gain,
    state,
    previous_keys,
    previous_values,
    previous_log_decay,
    previous_strengths,
    accepted,
    parent,
):
    gathered = lax.all_gather(tokens, ("kv", "tp"), axis=2, tiled=True)
    sequence_count, proposal_count, width = gathered.shape
    row_total = sequence_count * proposal_count
    features = gathered.astype(jnp.float32)
    normed = features * lax.rsqrt(jnp.mean(features * features, axis=-1, keepdims=True) + epsilon)
    normed = (normed * input_norm_gain.astype(jnp.float32)).astype(jnp.bfloat16)
    flat_rows = normed.reshape(row_total, width)
    write_strength_logits = jnp.dot(flat_rows, strength_weight, preferred_element_type=jnp.float32)
    decay_logits = jnp.dot(flat_rows, decay_weight, preferred_element_type=jnp.float32)
    value_projected = jnp.dot(
        flat_rows, value_weight.reshape(width, -1), preferred_element_type=jnp.float32
    ).astype(jnp.bfloat16)
    output_gate_logits = jnp.dot(
        flat_rows, output_gate_weight.reshape(width, -1), preferred_element_type=jnp.float32
    ).astype(jnp.bfloat16)
    query_projected = jnp.dot(flat_rows, query_weight, preferred_element_type=jnp.float32).astype(
        jnp.bfloat16
    )
    key_projected = jnp.dot(flat_rows, key_weight, preferred_element_type=jnp.float32).astype(
        jnp.bfloat16
    )
    blended_rows, accepted_state = delta_recursion(
        query_projected,
        key_projected,
        value_projected,
        output_gate_logits,
        write_strength_logits,
        decay_logits,
        head_decay_rate,
        proposal_log_decay,
        head_norm_gain,
        state,
        previous_keys,
        previous_values,
        previous_log_decay,
        previous_strengths,
        accepted,
        parent,
        channel_sum,
    )
    partial_out = jnp.dot(
        blended_rows, output_weight.reshape(-1, width), preferred_element_type=jnp.float32
    )
    own_cols = output_norm_gain.shape[0]
    totals = lax.psum(partial_out, ("kv", "tp"))
    scaling = lax.rsqrt(jnp.mean(totals * totals, axis=-1, keepdims=True) + epsilon)
    own_index = lax.axis_index("kv") * lax.axis_size("tp") + lax.axis_index("tp")
    share = lax.dynamic_slice_in_dim(totals, own_index * own_cols, own_cols, 1)
    layer_out = (share * scaling * output_norm_gain.astype(jnp.float32)).astype(jnp.bfloat16)
    return (layer_out.reshape(sequence_count, proposal_count, own_cols), accepted_state)


def solution(mesh):
    placed = (
        P(None, None, ("kv", "tp")),
        P(),
        P(None, "kv"),
        P(None, "kv"),
        P(None, "kv", "tp"),
        P(None, "kv", "tp"),
        P(None, "kv"),
        P(None, "kv"),
        P("kv"),
        P(None, None, "kv"),
        P("tp"),
        P("kv", "tp", None),
        P(("kv", "tp")),
        P(None, "kv", "tp", None),
        P(None, None, "kv"),
        P(None, None, "kv", "tp"),
        P(None, None, "kv"),
        P(None, None, "kv"),
        P(),
        P(),
    )
    return jax.shard_map(
        on_device,
        mesh=mesh,
        in_specs=placed,
        out_specs=(P(None, None, ("kv", "tp")), P(None, "kv", "tp", None)),
        check_vma=False,
    )
```

profile of v0, /device:TPU:0, one launch (start us, length us, event | category | flops | bytes accessed | tf_op | source)
XLA Modules:
  0.0 489.5 jit_solution(4462959712660813374)
XLA Ops:
  17.7 58.3 %all-gather.2.cloned.1.call-done = bf16[256,4,2048]{0,2,1:T(8,128)(2,1)} async-done(((bf16[256,4,64]{0,2,1:T(8,128)(2,1)}), bf16[256,4,2048]{0,2,1:T(8,128)(2,1)}) %all-gather.2.cloned.1.call-update) | async-done | bytes 4194320 | tf_op jit(solution)/shard_map/all_gather | solution.py:174
  76.1 3.2 fusion
  79.5 2.7 fusion.2
  82.2 7.9 %copy.594 = bf16[256,4,2048]{2,1,0:T(4,128)(2,1)} copy(bf16[256,4,2048]{0,2,1:T(8,128)(2,1)} %fusion.2) | data formatting | bytes 8388608 | tf_op jit(solution)/shard_map/convert_element_type | solution.py:179
  90.2 3.0 fusion.61
  98.4 6.9 %reshape.134 = bf16[1024,2048]{1,0:T(8,128)(2,1)} reshape(bf16[256,4,2048]{2,1,0:T(4,128)(2,1)} %copy.594) | data formatting | bytes 8388608 | tf_op jit(solution)/shard_map/reshape | solution.py:180
  105.2 3.4 fusion.9
  115.3 5.3 %multiply_multiply_fusion = f32[256,2,8,8]{3,2,1,0:T(8,128)S(1)} fusion(f32[256,2,4,128]{3,2,1,0:T(4,128)S(1)} %bitcast_multiply_fusion, f32[256,2,4,128]{3,2,1,0:T(4,128)S(1)} %fusion.16, f32[256,8,8]{2,1,0:T(8,128)S(1)} %copy-done.22, f32[256,2,8]{2,1,0:T(2,128)} %copy.621, f32[256,2,8]{2,1,0:T(2,128)S(1)} %copy.615), kind=kOutput, calls=%fused_computation.26 | convolution fusion | flops 51019776 | bytes 2326528 | tf_op jit(solution)/shard_map/bhid,bhjd->bhij/dot_general | solution.py:14
  128.1 3.4 fusion.10
  133.5 15.6 %fusion.22 = f32[256,2,4,32]{3,2,1,0:T(4,128)S(1)} fusion(f32[256,2,32,128]{3,2,1,0:T(8,128)} %param.33, f32[256,4,2,128]{3,2,1,0:T(2,128)S(1)} %reshape.152, f32[256,2,4]{2,1,0:T(2,128)S(1)} %copy.609, f32[256,2,4]{2,1,0:T(2,128)S(1)} %copy.597), kind=kOutput, calls=%fused_computation.58 | convolution fusion | flops 101187584 | bytes 9715712 | tf_op jit(solution)/shard_map/bhid,bhed->bhie/dot_general | solution.py:14
  157.2 10.5 %pad_maximum_fusion.7 = (f32[256,2,1,160]{3,2,1,0:T(1,128)}, f32[256,2,1,160]{3,2,1,0:T(1,128)S(1)}, f32[256,2,1,160]{3,2,1,0:T(1,128)S(1)}, f32[256,2,1,160]{3,...) fusion(f32[256,2,8,128]{3,2,1,0:T(8,128)S(1)} %fusion.8, ...), kind=kLoop, calls=%fused_computation.72 | loop fusion | flops 655360 | bytes 5242880 | tf_op jit(solution)/shard_map/concatenate | solution.py:109
  170.8 7.6 %fusion.24 = f32[256,2,1,160]{3,2,1,0:T(1,128)} fusion(f32[256,2,1,160]{3,2,1,0:T(1,128)S(1)} %copy.650, f32[256,2,1,160]{3,2,1,0:T(1,128)S(1)} %get-tuple-element.41, f32[256,2,8,8]{3,2,1,0:T(8,128)} %copy-done.6), kind=kOutput, calls=%fused_computation.60 | convolution fusion | flops 2129920 | bytes 1245184 | tf_op jit(solution)/shard_map/bhj,bhjd->bhd/dot_general | solution.py:14
  188.9 8.4 %fusion.5 = f32[256,2,1,160]{3,2,1,0:T(1,128)} fusion(f32[256,2,1,160]{3,2,1,0:T(1,128)} %copy.652, f32[256,2,1,160]{3,2,1,0:T(1,128)} %copy.651, f32[256,2,1,160]{3,2,1,0:T(1,128)} %copy-done.8, f32[256,2,1,160]{3,2,1,0:T(1,128)S(1)} %get-tuple-element.41, f32[256,2,8,8]{3,2,1,0:T(8,128)S(1)} %copy-done.7), kind=kOutput, calls=%fused_computation.28 | convolution fusion | flops 4915200 | bytes 2097152 | tf_op jit(solution)/shard_map/bhj,bhjd->bhd/dot_general | solution.py:14
  220.7 11.4 %stack.101 = f32[256,2,7,160]{3,2,1,0:T(8,128)} concatenate(f32[256,2,1,160]{3,2,1,0:T(1,128)S(1)} %get-tuple-element.41, f32[256,2,1,160]{3,2,1,0:T(1,128)S(1)} %copy-done.9, f32[256,2,1,160]{3,2,1,0:T(1,128)} %copy.651, f32[256,2,1,160]{3,2,1,0:T(1,128)} %copy.652, f32[256,2,1,160]{3,2,1,0:T(1,128)} %copy.653, f32[256,2,1,160]{3,2,1,0:T(1,128)} %copy.654, f32[256,2,1,160]{3,2,1,0:T(1,128)} %copy.655), dimensions={2} | concatenate | bytes 4587520 | tf_op jit(solution)/shard_map/stack | solution.py:118
  232.2 7.2 %fusion.48 = f32[256,2,1,160]{3,2,1,0:T(1,128)} fusion(f32[256,2,7,160]{3,2,1,0:T(8,128)} %stack.101, f32[256,2,8,8]{3,2,1,0:T(8,128)S(1)} %copy-done.7), kind=kOutput, calls=%fused_computation.96 | convolution fusion | flops 6881280 | bytes 2883584 | tf_op jit(solution)/shard_map/bhj,bhjd->bhd/dot_general | solution.py:14
  246.2 11.2 %stack.103 = f32[256,2,8,160]{3,2,1,0:T(8,128)} concatenate(f32[256,2,1,160]{3,2,1,0:T(1,128)S(1)} %get-tuple-element.41, f32[256,2,1,160]{3,2,1,0:T(1,128)S(1)} %copy-done.9, f32[256,2,1,160]{3,2,1,0:T(1,128)S(1)} %copy-done.10, f32[256,2,1,160]{3,2,1,0:T(1,128)S(1)} %copy-done.11, f32[256,2,1,160]{3,2,1,0:T(1,128)S(1)} %copy-done.12, f32[256,2,1,160]{3,2,1,0:T(1,128)S(1)} %copy-done.13, ...), dimensions={2} | concatenate | bytes 5242880 | tf_op jit(solution)/shard_map/stack | solution.py:121
  257.4 16.8 %slice_subtract_fusion = f32[256,2,8,32]{3,2,1,0:T(8,128)S(1)} fusion(f32[256,2,8,160]{3,2,1,0:T(8,128)} %stack.103, f32[256,2,32,128]{3,2,1,0:T(8,128)} %param.33), kind=kOutput, calls=%fused_computation.23 | convolution fusion | flops 201457664 | bytes 11534336 | tf_op jit(solution)/shard_map/bhcd,bhed->bhce/dot_general | solution.py:14
  274.3 4.2 convolution_multiply_fusion
  278.6 3.4 fusion.95
  284.3 6.4 %psum.14 = f32[256,2,4]{0,2,1:T(4,128)S(1)} all-reduce(f32[256,2,4]{0,2,1:T(4,128)S(1)} %copy.659), channel_id=1, replica_groups=mesh['kv'=8,'tp'=4] {'tp'}, use_global_device_ids=true, to_apply=%region_5.6 | all-reduce | flops 2048 | bytes 16384 | tf_op jit(solution)/shard_map/psum | solution.py:149
  292.8 4.5 fusion.96
  298.4 18.9 %multiply_add_fusion = f32[256,2,32,128]{3,2,1,0:T(8,128)} fusion(f32[256,2,32,128]{3,2,1,0:T(8,128)} %param.33, f32[256,2]{1,0:T(8,128)S(1)} %bitcast.222, f32[256,2,8,32]{3,2,1,0:T(8,128)S(1)} %slice_subtract_fusion, f32[256,2,4]{2,1,0:T(2,128)S(1)} %copy.666, bf16[256,4,256]{2,1,0:T(4,128)(2,1)S(1)} %copy-done.26, f32[256,2,4]{2,1,0:T(2,128)S(1)} %copy-done.32), kind=kOutput, calls=%fused_computation.19 | convolution fusion | flops 105644032 | bytes 19005440 | tf_op jit(solution)/shard_map/bhcd,bhce->bhed/dot_general | solution.py:14
  317.2 158.6 %all-reduce.4.cloned.1.call-done = f32[1024,2048]{1,0:T(8,128)} async-done(((f32[1024,2048]{1,0:T(8,128)}), f32[1024,2048]{1,0:T(8,128)}) %all-reduce.4.cloned.1.call-update) | async-done | bytes 8388624 | tf_op jit(solution)/shard_map/psum | solution.py:218
  475.8 4.1 multiply_reduce_fusion
  (226 shorter events, 91.0 us)
Async XLA Ops:
  7.2 98.1 %copy-start = (bf16[2048,256]{1,0:T(8,128)(2,1)S(1)}, bf16[2048,256]{1,0:T(8,128)(2,1)}, u32[]{:S(2)}) copy-start(bf16[2048,256]{1,0:T(8,128)(2,1)} %param.23) | copy-start | bytes 3145732
  7.2 7.7 %copy-start.41 = (bf16[256,4,2,32]{0,3,2,1:T(8,128)(2,1)S(1)}, bf16[256,4,2,32]{0,3,2,1:T(8,128)(2,1)}, u32[]{:S(2)}) copy-start(bf16[256,4,2,32]{0,3,2,1:T(8,128)(2,1)} %param.35) | copy-start | bytes 393220
  7.2 8.8 %copy-start.47 = (s32[256]{0:T(256)S(1)}, s32[256]{0:T(256)}, u32[]{:S(2)}) copy-start(s32[256]{0:T(256)} %param.38) | copy-start | bytes 3076
  7.2 8.8 %copy-start.44 = (f32[256,4,2]{0,2,1:T(2,128)S(1)}, f32[256,4,2]{0,2,1:T(2,128)}, u32[]{:S(2)}) copy-start(f32[256,4,2]{0,2,1:T(2,128)} %param.36) | copy-start | bytes 24580
  7.2 8.8 %copy-start.45 = (f32[256,4,2]{0,2,1:T(2,128)S(1)}, f32[256,4,2]{0,2,1:T(2,128)}, u32[]{:S(2)}) copy-start(f32[256,4,2]{0,2,1:T(2,128)} %param.37) | copy-start | bytes 24580
  7.2 68.8 %all-gather.2.cloned.1.call-start = ((), (), s32[]{:S(2)}) async-start(), calls=%async_computation | async-start | bytes 4325376 | tf_op jit(solution)/shard_map/all_gather | solution.py:174
  8.0 467.8 %all-reduce.4.cloned.1.call-start = ((), (), s32[]{:S(2)}) async-start(), calls=%async_computation.1 | async-start | bytes 16777216 | tf_op jit(solution)/shard_map/psum | solution.py:218
  11.4 83.1 %copy-start.21 = (f32[256,8,8]{2,1,0:T(8,128)}, f32[256,8,8]{2,1,0:T(8,128)S(1)}, u32[]{:S(2)}) copy-start(f32[256,8,8]{2,1,0:T(8,128)S(1)} %copy.607) | copy-start | bytes 196612
  13.9 65.3 %copy-start.31 = (f32[256,2,4]{2,1,0:T(2,128)}, f32[256,2,4]{2,1,0:T(2,128)S(1)}, u32[]{:S(2)}) copy-start(f32[256,2,4]{2,1,0:T(2,128)S(1)} %copy.611) | copy-start | bytes 24580
  17.7 97.6 %copy-start.14 = (f32[256,2,4,128]{3,2,1,0:T(4,128)}, f32[256,2,4,128]{3,2,1,0:T(4,128)S(1)}, u32[]{:S(2)}) copy-start(f32[256,2,4,128]{3,2,1,0:T(4,128)S(1)} %fusion.16) | copy-start | bytes 3145732
  82.2 7.9 %copy-start.42 = (bf16[2048,2]{0,1:T(2,128)(2,1)S(1)}, bf16[2048,2]{0,1:T(2,128)(2,1)}, u32[]{:S(2)}) copy-start(bf16[2048,2]{0,1:T(2,128)(2,1)} %param.27) | copy-start | bytes 24580
  112.8 7.9 %copy-start.17 = (f32[256,2,4,128]{3,2,1,0:T(4,128)}, f32[256,2,4,128]{3,2,1,0:T(4,128)S(1)}, u32[]{:S(2)}) copy-start(f32[256,2,4,128]{3,2,1,0:T(4,128)S(1)} %bitcast_multiply_fusion) | copy-start | bytes 3145732
  115.3 9.1 %copy-start.3 = (bf16[1024,2048]{1,0:T(8,128)(2,1)S(1)}, bf16[1024,2048]{1,0:T(8,128)(2,1)}, u32[]{:S(2)}) copy-start(bf16[1024,2048]{1,0:T(8,128)(2,1)} %reshape.134) | copy-start | bytes 12582916
  133.5 15.6 %copy-start.39 = (f32[256,2,4]{2,1,0:T(2,128)}, f32[256,2,4]{2,1,0:T(2,128)S(1)}, u32[]{:S(2)}) copy-start(f32[256,2,4]{2,1,0:T(2,128)S(1)} %copy.597) | copy-start | bytes 24580
  157.2 11.8 %copy-start.34 = (f32[256,2,1,1]{3,2,1,0:T(1,128)S(1)}, f32[256,2,1,1]{3,2,1,0:T(1,128)}, u32[]{:S(2)}) copy-start(f32[256,2,1,1]{3,2,1,0:T(1,128)} %slice.141) | copy-start | bytes 6148
  170.8 7.6 %copy-start.8 = (f32[256,2,1,160]{3,2,1,0:T(1,128)}, f32[256,2,1,160]{3,2,1,0:T(1,128)S(1)}, u32[]{:S(2)}) copy-start(f32[256,2,1,160]{3,2,1,0:T(1,128)S(1)} %copy.650) | copy-start | bytes 983044
  170.8 8.9 %copy-start.29 = (f32[256,2,1,160]{3,2,1,0:T(1,128)S(1)}, f32[256,2,1,160]{3,2,1,0:T(1,128)}, u32[]{:S(2)}) copy-start(f32[256,2,1,160]{3,2,1,0:T(1,128)} %get-tuple-element.43) | copy-start | bytes 983044
  257.3 16.9 %copy-start.16 = (f32[256,2,4,128]{3,2,1,0:T(4,128)S(1)}, f32[256,2,4,128]{3,2,1,0:T(4,128)}, u32[]{:S(2)}) copy-start(f32[256,2,4,128]{3,2,1,0:T(4,128)} %copy-done.14) | copy-start | bytes 3145732
  257.4 16.9 %copy-start.18 = (f32[256,2,4,128]{3,2,1,0:T(4,128)S(1)}, f32[256,2,4,128]{3,2,1,0:T(4,128)}, u32[]{:S(2)}) copy-start(f32[256,2,4,128]{3,2,1,0:T(4,128)} %copy-done.17) | copy-start | bytes 3145732
  257.4 16.9 %copy-start.20 = (f32[256,4,2,128]{3,2,1,0:T(2,128)S(1)}, f32[256,4,2,128]{3,2,1,0:T(2,128)}, u32[]{:S(2)}) copy-start(f32[256,4,2,128]{3,2,1,0:T(2,128)} %copy-done.19) | copy-start | bytes 3145732
  257.4 16.9 %copy-start.25 = (f32[256,2,8,8]{3,2,1,0:T(8,128)S(1)}, f32[256,2,8,8]{3,2,1,0:T(8,128)}, u32[]{:S(2)}) copy-start(f32[256,2,8,8]{3,2,1,0:T(8,128)} %broadcast_subtract_fusion) | copy-start | bytes 393220
  257.4 16.9 %copy-start.35 = (f32[256,4,8]{2,1,0:T(4,128)S(1)}, f32[256,4,8]{2,1,0:T(4,128)}, u32[]{:S(2)}) copy-start(f32[256,4,8]{2,1,0:T(4,128)} %copy.617) | copy-start | bytes 98308
  257.4 16.9 %copy-start.40 = (f32[256,2,4]{2,1,0:T(2,128)S(1)}, f32[256,2,4]{2,1,0:T(2,128)}, u32[]{:S(2)}) copy-start(f32[256,2,4]{2,1,0:T(2,128)} %copy-done.39) | copy-start | bytes 24580
  283.2 9.6 %copy-start.38 = (bf16[2,32,2048]{2,1,0:T(8,128)(2,1)S(1)}, bf16[2,32,2048]{2,1,0:T(8,128)(2,1)}, u32[]{:S(2)}) copy-start(bf16[2,32,2048]{2,1,0:T(8,128)(2,1)} %param.31) | copy-start | bytes 786436
  (28 other events, 99.4 us)
Sparse Core Ops, SparseCore 0:
  10.9 65.0 all-gather.1
  297.4 178.3 all-reduce.3
where the time goes:
time: 496 us; the launch traced here: 489 us
  waiting for transfers between devices  218 us (44%)
  matrix products  108 us (22%)
  local copies, waits for them, and re-layouts  89.5 us (18%)
  other arithmetic  52.6 us (11%)
  between operations  15.5 us (3%)
  blocking collectives  6.36 us (1%)
    psum x1, waiting for transfers between devices, on_device(): totals = lax.psum(partial_out, ('kv', 'tp'))  159 us
    dot_general x10, matrix products, exact_product(): return jnp.einsum(form, left, right, precision=lax.Precision.HIGHEST)  90 us
    all_gather x1, waiting for transfers between devices, on_device(): gathered = lax.all_gather(tokens, ('kv', 'tp'), axis=2, tiled=True)  58.3 us
    another operation x8, local copies, waits for them, and re-layouts, delta_recursion(): solution = jnp.stack(solved, axis=2)  22.3 us
    another operation x2, local copies, waits for them, and re-layouts, delta_recursion(): jnp.stack(solved, axis=2)  12.1 us
    unnamed x110, local copies, waits for them, and re-layouts  11 us
    concatenate x1, other arithmetic, delta_recursion(): jnp.concatenate([beta_all[..., None] * values_all, (beta_all * jnp.exp(ga...  10.5 us
  transfers between devices with their start and end apart: 2, of which 2 were waited for; matrix products, arithmetic and copies ran while one was open for 6% of the time, Pallas kernels for 0%

commit v1 on v0

--- a/solution.py
+++ b/solution.py
@@ -215,7 +215,7 @@
         blended_rows, output_weight.reshape(-1, width), preferred_element_type=jnp.float32
     )
     own_cols = output_norm_gain.shape[0]
-    totals = lax.psum(partial_out, ("kv", "tp"))
+    totals = lax.psum(lax.psum(partial_out, "tp"), "kv")
     scaling = lax.rsqrt(jnp.mean(totals * totals, axis=-1, keepdims=True) + epsilon)
     own_index = lax.axis_index("kv") * lax.axis_size("tp") + lax.axis_index("tp")
     share = lax.dynamic_slice_in_dim(totals, own_index * own_cols, own_cols, 1)

time: 496 us -> 744 us (1.50)
  waiting for transfers between devices: 218 us -> 465 us
    psum x1 -> x2, waiting for transfers between devices: 159 us -> 406 us  [on_device(): totals = lax.psum(lax.psum(partial_out, 'tp'), 'kv')]
  transfers between devices with their start and end apart: 2 -> 3, of which waited for: 2 -> 3; matrix products, arithmetic and copies ran while one was open for 6% -> 4% of each run, Pallas kernels for 0% -> 0%
where the time goes in v1:
time: 744 us; the launch traced here: 737 us
  waiting for transfers between devices  465 us (62%)
  matrix products  108 us (15%)
  local copies, waits for them, and re-layouts  89.2 us (12%)
  other arithmetic  52.6 us (7%)
  between operations  15.2 us (2%)
    psum x2, waiting for transfers between devices, on_device(): totals = lax.psum(lax.psum(partial_out, 'tp'), 'kv')  406 us
    dot_general x10, matrix products, exact_product(): return jnp.einsum(form, left, right, precision=lax.Precision.HIGHEST)  90.3 us
    all_gather x1, waiting for transfers between devices, on_device(): gathered = lax.all_gather(tokens, ('kv', 'tp'), axis=2, tiled=True)  58.3 us
    another operation x8, local copies, waits for them, and re-layouts, delta_recursion(): solution = jnp.stack(solved, axis=2)  22.3 us
  transfers between devices with their start and end apart: 3, of which 3 were waited for; matrix products, arithmetic and copies ran while one was open for 4% of the time, Pallas kernels for 0%

profile of v1, /device:TPU:0, one launch (start us, length us, event | category | flops | bytes accessed | tf_op | source)
XLA Modules:
  0.0 736.9 jit_solution(17001707705488860015)
XLA Ops:
  17.7 58.3 %all-gather.2.cloned.1.call-done = bf16[256,4,2048]{0,2,1:T(8,128)(2,1)} async-done(((bf16[256,4,64]{0,2,1:T(8,128)(2,1)}), bf16[256,4,2048]{0,2,1:T(8,128)(2,1)}) %all-gather.2.cloned.1.call-update) | async-done | bytes 4194320 | tf_op jit(solution)/shard_map/all_gather | solution.py:174
  76.1 3.2 fusion
  82.2 7.9 %copy.594 = bf16[256,4,2048]{2,1,0:T(4,128)(2,1)} copy(bf16[256,4,2048]{0,2,1:T(8,128)(2,1)} %fusion.2) | data formatting | bytes 8388608 | tf_op jit(solution)/shard_map/convert_element_type | solution.py:179
  90.2 3.0 fusion.61
  98.4 6.9 reshape.134
  105.2 3.4 fusion.9
  115.3 5.3 multiply_multiply_fusion
  128.1 3.4 fusion.10
  133.5 15.6 %fusion.22 = f32[256,2,4,32]{3,2,1,0:T(4,128)S(1)} fusion(f32[256,2,32,128]{3,2,1,0:T(8,128)} %param.33, f32[256,4,2,128]{3,2,1,0:T(2,128)S(1)} %reshape.152, f32[256,2,4]{2,1,0:T(2,128)S(1)} %copy.609, f32[256,2,4]{2,1,0:T(2,128)S(1)} %copy.597), kind=kOutput, calls=%fused_computation.58 | convolution fusion | flops 101187584 | bytes 9715712 | tf_op jit(solution)/shard_map/bhid,bhed->bhie/dot_general | solution.py:14
  157.2 10.5 %pad_maximum_fusion.7 = (f32[256,2,1,160]{3,2,1,0:T(1,128)}, f32[256,2,1,160]{3,2,1,0:T(1,128)S(1)}, f32[256,2,1,160]{3,2,1,0:T(1,128)S(1)}, f32[256,2,1,160]{3,...) fusion(f32[256,2,8,128]{3,2,1,0:T(8,128)S(1)} %fusion.8, ...), kind=kLoop, calls=%fused_computation.72 | loop fusion | flops 655360 | bytes 5242880 | tf_op jit(solution)/shard_map/concatenate | solution.py:109
  170.8 7.6 %fusion.24 = f32[256,2,1,160]{3,2,1,0:T(1,128)} fusion(f32[256,2,1,160]{3,2,1,0:T(1,128)S(1)} %copy.650, f32[256,2,1,160]{3,2,1,0:T(1,128)S(1)} %get-tuple-element.41, f32[256,2,8,8]{3,2,1,0:T(8,128)} %copy-done.6), kind=kOutput, calls=%fused_computation.60 | convolution fusion | flops 2129920 | bytes 1245184 | tf_op jit(solution)/shard_map/bhj,bhjd->bhd/dot_general | solution.py:14
  188.9 8.4 %fusion.5 = f32[256,2,1,160]{3,2,1,0:T(1,128)} fusion(f32[256,2,1,160]{3,2,1,0:T(1,128)} %copy.652, f32[256,2,1,160]{3,2,1,0:T(1,128)} %copy.651, f32[256,2,1,160]{3,2,1,0:T(1,128)} %copy-done.8, f32[256,2,1,160]{3,2,1,0:T(1,128)S(1)} %get-tuple-element.41, f32[256,2,8,8]{3,2,1,0:T(8,128)S(1)} %copy-done.7), kind=kOutput, calls=%fused_computation.28 | convolution fusion | flops 4915200 | bytes 2097152 | tf_op jit(solution)/shard_map/bhj,bhjd->bhd/dot_general | solution.py:14
  220.7 11.4 %stack.101 = f32[256,2,7,160]{3,2,1,0:T(8,128)} concatenate(f32[256,2,1,160]{3,2,1,0:T(1,128)S(1)} %get-tuple-element.41, f32[256,2,1,160]{3,2,1,0:T(1,128)S(1)} %copy-done.9, f32[256,2,1,160]{3,2,1,0:T(1,128)} %copy.651, f32[256,2,1,160]{3,2,1,0:T(1,128)} %copy.652, f32[256,2,1,160]{3,2,1,0:T(1,128)} %copy.653, f32[256,2,1,160]{3,2,1,0:T(1,128)} %copy.654, f32[256,2,1,160]{3,2,1,0:T(1,128)} %copy.655), dimensions={2} | concatenate | bytes 4587520 | tf_op jit(solution)/shard_map/stack | solution.py:118
  232.2 7.2 fusion.48
  246.2 11.2 %stack.103 = f32[256,2,8,160]{3,2,1,0:T(8,128)} concatenate(f32[256,2,1,160]{3,2,1,0:T(1,128)S(1)} %get-tuple-element.41, f32[256,2,1,160]{3,2,1,0:T(1,128)S(1)} %copy-done.9, f32[256,2,1,160]{3,2,1,0:T(1,128)S(1)} %copy-done.10, f32[256,2,1,160]{3,2,1,0:T(1,128)S(1)} %copy-done.11, f32[256,2,1,160]{3,2,1,0:T(1,128)S(1)} %copy-done.12, f32[256,2,1,160]{3,2,1,0:T(1,128)S(1)} %copy-done.13, ...), dimensions={2} | concatenate | bytes 5242880 | tf_op jit(solution)/shard_map/stack | solution.py:121
  257.4 16.8 %slice_subtract_fusion = f32[256,2,8,32]{3,2,1,0:T(8,128)S(1)} fusion(f32[256,2,8,160]{3,2,1,0:T(8,128)} %stack.103, f32[256,2,32,128]{3,2,1,0:T(8,128)} %param.33), kind=kOutput, calls=%fused_computation.23 | convolution fusion | flops 201457664 | bytes 11534336 | tf_op jit(solution)/shard_map/bhcd,bhed->bhce/dot_general | solution.py:14
  274.3 4.2 convolution_multiply_fusion
  278.6 3.4 fusion.95
  284.3 6.4 psum.21
  292.5 4.6 fusion.96
  297.2 152.4 %all-reduce.5.cloned.1.call-done = f32[1024,2048]{1,0:T(8,128)} async-done(((f32[1024,2048]{1,0:T(8,128)}), f32[1024,2048]{1,0:T(8,128)}) %all-reduce.5.cloned.1.call-update) | async-done | bytes 8388624 | tf_op jit(solution)/shard_map/psum | solution.py:218
  450.7 19.1 %multiply_add_fusion = f32[256,2,32,128]{3,2,1,0:T(8,128)} fusion(f32[256,2,32,128]{3,2,1,0:T(8,128)} %param.33, f32[256,2]{1,0:T(8,128)S(1)} %bitcast.222, f32[256,2,8,32]{3,2,1,0:T(8,128)S(1)} %slice_subtract_fusion, f32[256,2,4]{2,1,0:T(2,128)S(1)} %copy.666, bf16[256,4,256]{2,1,0:T(4,128)(2,1)S(1)} %copy-done.26, f32[256,2,4]{2,1,0:T(2,128)S(1)} %copy-done.32), kind=kOutput, calls=%fused_computation.19 | convolution fusion | flops 105644032 | bytes 19005440 | tf_op jit(solution)/shard_map/bhcd,bhce->bhed/dot_general | solution.py:14
  469.8 253.8 %all-reduce.7.cloned.1.call-done = f32[1024,2048]{1,0:T(8,128)} async-done(((f32[1024,2048]{1,0:T(8,128)}), f32[1024,2048]{1,0:T(8,128)}) %all-reduce.7.cloned.1.call-update) | async-done | bytes 8388624 | tf_op jit(solution)/shard_map/psum | solution.py:218
  723.6 4.1 multiply_reduce_fusion
  (229 shorter events, 93.5 us)
Async XLA Ops:
  7.2 98.1 %copy-start = (bf16[2048,256]{1,0:T(8,128)(2,1)S(1)}, bf16[2048,256]{1,0:T(8,128)(2,1)}, u32[]{:S(2)}) copy-start(bf16[2048,256]{1,0:T(8,128)(2,1)} %param.23) | copy-start | bytes 3145732
  7.2 7.7 %copy-start.41 = (bf16[256,4,2,32]{0,3,2,1:T(8,128)(2,1)S(1)}, bf16[256,4,2,32]{0,3,2,1:T(8,128)(2,1)}, u32[]{:S(2)}) copy-start(bf16[256,4,2,32]{0,3,2,1:T(8,128)(2,1)} %param.35) | copy-start | bytes 393220
  7.2 8.8 %copy-start.47 = (s32[256]{0:T(256)S(1)}, s32[256]{0:T(256)}, u32[]{:S(2)}) copy-start(s32[256]{0:T(256)} %param.38) | copy-start | bytes 3076
  7.2 8.8 %copy-start.44 = (f32[256,4,2]{0,2,1:T(2,128)S(1)}, f32[256,4,2]{0,2,1:T(2,128)}, u32[]{:S(2)}) copy-start(f32[256,4,2]{0,2,1:T(2,128)} %param.36) | copy-start | bytes 24580
  7.2 8.8 %copy-start.45 = (f32[256,4,2]{0,2,1:T(2,128)S(1)}, f32[256,4,2]{0,2,1:T(2,128)}, u32[]{:S(2)}) copy-start(f32[256,4,2]{0,2,1:T(2,128)} %param.37) | copy-start | bytes 24580
  7.2 68.8 %all-gather.2.cloned.1.call-start = ((), (), s32[]{:S(2)}) async-start(), calls=%async_computation | async-start | bytes 4325376 | tf_op jit(solution)/shard_map/all_gather | solution.py:174
  8.0 441.6 %all-reduce.5.cloned.1.call-start = ((), (), s32[]{:S(2)}) async-start(), calls=%async_computation.1 | async-start | bytes 16777216 | tf_op jit(solution)/shard_map/psum | solution.py:218
  11.4 83.1 %copy-start.21 = (f32[256,8,8]{2,1,0:T(8,128)}, f32[256,8,8]{2,1,0:T(8,128)S(1)}, u32[]{:S(2)}) copy-start(f32[256,8,8]{2,1,0:T(8,128)S(1)} %copy.607) | copy-start | bytes 196612
  13.9 65.3 %copy-start.31 = (f32[256,2,4]{2,1,0:T(2,128)}, f32[256,2,4]{2,1,0:T(2,128)S(1)}, u32[]{:S(2)}) copy-start(f32[256,2,4]{2,1,0:T(2,128)S(1)} %copy.611) | copy-start | bytes 24580
  17.7 97.6 %copy-start.14 = (f32[256,2,4,128]{3,2,1,0:T(4,128)}, f32[256,2,4,128]{3,2,1,0:T(4,128)S(1)}, u32[]{:S(2)}) copy-start(f32[256,2,4,128]{3,2,1,0:T(4,128)S(1)} %fusion.16) | copy-start | bytes 3145732
  82.2 7.9 %copy-start.42 = (bf16[2048,2]{0,1:T(2,128)(2,1)S(1)}, bf16[2048,2]{0,1:T(2,128)(2,1)}, u32[]{:S(2)}) copy-start(bf16[2048,2]{0,1:T(2,128)(2,1)} %param.27) | copy-start | bytes 24580
  112.8 7.9 %copy-start.17 = (f32[256,2,4,128]{3,2,1,0:T(4,128)}, f32[256,2,4,128]{3,2,1,0:T(4,128)S(1)}, u32[]{:S(2)}) copy-start(f32[256,2,4,128]{3,2,1,0:T(4,128)S(1)} %bitcast_multiply_fusion) | copy-start | bytes 3145732
  115.3 9.1 %copy-start.3 = (bf16[1024,2048]{1,0:T(8,128)(2,1)S(1)}, bf16[1024,2048]{1,0:T(8,128)(2,1)}, u32[]{:S(2)}) copy-start(bf16[1024,2048]{1,0:T(8,128)(2,1)} %reshape.134) | copy-start | bytes 12582916
  133.5 15.6 %copy-start.39 = (f32[256,2,4]{2,1,0:T(2,128)}, f32[256,2,4]{2,1,0:T(2,128)S(1)}, u32[]{:S(2)}) copy-start(f32[256,2,4]{2,1,0:T(2,128)S(1)} %copy.597) | copy-start | bytes 24580
  157.2 11.8 %copy-start.34 = (f32[256,2,1,1]{3,2,1,0:T(1,128)S(1)}, f32[256,2,1,1]{3,2,1,0:T(1,128)}, u32[]{:S(2)}) copy-start(f32[256,2,1,1]{3,2,1,0:T(1,128)} %slice.141) | copy-start | bytes 6148
  170.8 8.9 %copy-start.29 = (f32[256,2,1,160]{3,2,1,0:T(1,128)S(1)}, f32[256,2,1,160]{3,2,1,0:T(1,128)}, u32[]{:S(2)}) copy-start(f32[256,2,1,160]{3,2,1,0:T(1,128)} %get-tuple-element.43) | copy-start | bytes 983044
  257.3 16.9 %copy-start.16 = (f32[256,2,4,128]{3,2,1,0:T(4,128)S(1)}, f32[256,2,4,128]{3,2,1,0:T(4,128)}, u32[]{:S(2)}) copy-start(f32[256,2,4,128]{3,2,1,0:T(4,128)} %copy-done.14) | copy-start | bytes 3145732
  257.4 16.9 %copy-start.18 = (f32[256,2,4,128]{3,2,1,0:T(4,128)S(1)}, f32[256,2,4,128]{3,2,1,0:T(4,128)}, u32[]{:S(2)}) copy-start(f32[256,2,4,128]{3,2,1,0:T(4,128)} %copy-done.17) | copy-start | bytes 3145732
  257.4 16.9 %copy-start.20 = (f32[256,4,2,128]{3,2,1,0:T(2,128)S(1)}, f32[256,4,2,128]{3,2,1,0:T(2,128)}, u32[]{:S(2)}) copy-start(f32[256,4,2,128]{3,2,1,0:T(2,128)} %copy-done.19) | copy-start | bytes 3145732
  257.4 16.9 %copy-start.25 = (f32[256,2,8,8]{3,2,1,0:T(8,128)S(1)}, f32[256,2,8,8]{3,2,1,0:T(8,128)}, u32[]{:S(2)}) copy-start(f32[256,2,8,8]{3,2,1,0:T(8,128)} %broadcast_subtract_fusion) | copy-start | bytes 393220
  257.4 16.9 %copy-start.35 = (f32[256,4,8]{2,1,0:T(4,128)S(1)}, f32[256,4,8]{2,1,0:T(4,128)}, u32[]{:S(2)}) copy-start(f32[256,4,8]{2,1,0:T(4,128)} %copy.617) | copy-start | bytes 98308
  257.4 16.9 %copy-start.40 = (f32[256,2,4]{2,1,0:T(2,128)S(1)}, f32[256,2,4]{2,1,0:T(2,128)}, u32[]{:S(2)}) copy-start(f32[256,2,4]{2,1,0:T(2,128)} %copy-done.39) | copy-start | bytes 24580
  283.2 9.3 %copy-start.38 = (bf16[2,32,2048]{2,1,0:T(8,128)(2,1)S(1)}, bf16[2,32,2048]{2,1,0:T(8,128)(2,1)}, u32[]{:S(2)}) copy-start(bf16[2,32,2048]{2,1,0:T(8,128)(2,1)} %param.31) | copy-start | bytes 786436
  297.1 426.5 %all-reduce.7.cloned.1.call-start = ((), (), s32[]{:S(2)}) async-start(), calls=%async_computation.2 | async-start | bytes 16777216 | tf_op jit(solution)/shard_map/psum | solution.py:218
  (29 other events, 107.1 us)
Sparse Core Ops, SparseCore 0:
  10.9 65.0 all-gather.1
  297.3 152.2 all-reduce.4
  453.4 270.1 all-reduce.6
